TPU v7x, 32 devices: a whole 2x2x4 slice. The times are simulated.
32 devices in a mesh: sp: 16 (over z, y, x), tp: 2 (over core).
Axes of the slice: x: 2, y: 2, z: 4, core: 2. Of those that a mesh axis runs over, the one named last changes fastest.
Arguments:
- queries: bfloat16 [2048, 1024], P('sp', 'tp'), may hold values from -6 to 6
- attn_out: bfloat16 [2048, 1024], P('sp', 'tp'), may hold values from -6 to 6
- out_grad: bfloat16 [2048, 1024], P('sp', 'tp'), may hold values from -384 to 384
- row_lse: float32 [2048, 8], P('sp', 'tp'), may hold values from 9.5 to 12.5
- source: bfloat16 [8192, 4096], P('sp', 'tp'), may hold values from -6 to 6
- saved_keys: bfloat16 [8192, 256], P('sp'), may hold values from -6 to 6
- saved_values: bfloat16 [8192, 256], P('sp'), may hold values from -6 to 6
- key_weight: bfloat16 [4096, 256], P('tp'), may hold values from -0.09375 to 0.09375
- value_weight: bfloat16 [4096, 256], P('tp'), may hold values from -0.09375 to 0.09375
Outputs:
- query_grad: float32 [2048, 1024], P('sp', 'tp')
- source_grad: float32 [8192, 4096], P('sp', 'tp')
- key_grad: float32 [256, 4096], P('sp', 'tp')
All inputs are finite; a program needn't handle non-finite values.
Results may differ from a plain program's by a relative error of at most 0.012.
Values may be sent and summed in bfloat16 or wider, within the bound.
A program may use at most 64 MiB of HBM per device.

v0:
```python
import math

import jax
import jax.numpy as jnp
from jax import lax
from jax.sharding import PartitionSpec as P

HEADS = 8
KV_HEADS = 2
HEAD_DIM = 128


def contract_rows(left, right):
    return lax.dot_general(
        left, right, (((0,), (0,)), ((), ())), preferred_element_type=jnp.float32
    )


def contract_cols(left, right):
    return lax.dot_general(
        left, right, (((1,), (1,)), ((), ())), preferred_element_type=jnp.float32
    )


def shards(
    queries, attn_out, out_grad, row_lse, source, saved_keys, saved_values, key_weight, value_weight
):
    local_heads = row_lse.shape[1]
    tgt_rows = queries.shape[0]
    width = queries.shape[1]
    src_rows = source.shape[0]
    sp_count = lax.axis_size("sp")
    first_head = lax.axis_index("tp") * local_heads
    per_key = HEADS // KV_HEADS
    score_scale = 1.0 / math.sqrt(HEAD_DIM)
    row_delta = jnp.sum(
        (out_grad.astype(jnp.float32) * attn_out.astype(jnp.float32)).reshape(
            tgt_rows, local_heads, HEAD_DIM
        ),
        axis=2,
    )
    row_blocks = jnp.stack([queries, out_grad])
    row_stats = jnp.stack([row_lse, row_delta])
    whole_stats = lax.all_gather(row_stats, "sp", axis=1, tiled=True)
    kv_starts = [(first_head + slot) // per_key * HEAD_DIM for slot in range(local_heads)]
    key_heads = [lax.dynamic_slice_in_dim(saved_keys, start, HEAD_DIM, 1) for start in kv_starts]
    value_heads = [
        lax.dynamic_slice_in_dim(saved_values, start, HEAD_DIM, 1) for start in kv_starts
    ]
    total_rows = tgt_rows * sp_count
    initial = (
        jnp.zeros((total_rows, width), jnp.float32),
        jnp.zeros((src_rows, KV_HEADS * HEAD_DIM), jnp.float32),
        jnp.zeros((src_rows, KV_HEADS * HEAD_DIM), jnp.float32),
    )
    whole_blocks = lax.all_gather(row_blocks, "sp", axis=1, tiled=True)
    rows = whole_blocks.shape[1]
    span = math.gcd(rows, 1024)
    count = rows // span

    def step(turn, inner):
        query_buf, key_acc, value_acc = inner
        begin = turn * span
        block_rows = lax.dynamic_slice_in_dim(whole_blocks, begin, span, 1)
        block_stats = lax.dynamic_slice_in_dim(whole_stats, begin, span, 1)
        parts = []
        for slot in range(local_heads):
            query_head = block_rows[0, :, slot * HEAD_DIM : (slot + 1) * HEAD_DIM]
            grad_head = block_rows[1, :, slot * HEAD_DIM : (slot + 1) * HEAD_DIM]
            lse_col = block_stats[0, :, slot : slot + 1]
            delta_col = block_stats[1, :, slot : slot + 1]
            scores = contract_cols(query_head, key_heads[slot]) * score_scale
            attn_probs = jnp.exp(scores - lse_col)
            dprobs = contract_cols(grad_head, value_heads[slot])
            dscores = (attn_probs * (dprobs - delta_col) * score_scale).astype(jnp.bfloat16)
            parts.append(jnp.dot(dscores, key_heads[slot], preferred_element_type=jnp.float32))
            key_part = contract_rows(dscores, query_head)
            value_part = contract_rows(attn_probs.astype(jnp.bfloat16), grad_head)
            kv_start = kv_starts[slot]
            key_acc = lax.dynamic_update_slice_in_dim(
                key_acc,
                lax.dynamic_slice_in_dim(key_acc, kv_start, HEAD_DIM, 1) + key_part,
                kv_start,
                1,
            )
            value_acc = lax.dynamic_update_slice_in_dim(
                value_acc,
                lax.dynamic_slice_in_dim(value_acc, kv_start, HEAD_DIM, 1) + value_part,
                kv_start,
                1,
            )
        query_buf = lax.dynamic_update_slice_in_dim(
            query_buf, jnp.concatenate(parts, axis=1), begin, 0
        )
        return (query_buf, key_acc, value_acc)

    partials, key_acc, value_acc = lax.fori_loop(0, count, step, initial)
    stacked = partials.reshape(sp_count, tgt_rows, width)
    received = lax.all_to_all(stacked, "sp", split_axis=0, concat_axis=0, tiled=True)
    query_grad = jnp.sum(received, axis=0)
    key_acc, value_acc = (
        lax.psum(key_acc.astype(jnp.bfloat16), "tp").astype(jnp.float32),
        lax.psum(value_acc.astype(jnp.bfloat16), "tp").astype(jnp.float32),
    )
    key_half = key_acc.astype(jnp.bfloat16)
    value_half = value_acc.astype(jnp.bfloat16)
    source_grad = contract_cols(key_half, key_weight) + contract_cols(value_half, value_weight)
    weight_scale = 1.0 / math.sqrt(src_rows * sp_count)
    key_grad = lax.psum_scatter(
        contract_rows(key_half, source) * weight_scale, "sp", scatter_dimension=0, tiled=True
    )
    return (query_grad, source_grad, key_grad)


def solution(mesh):
    in_specs = (
        P("sp", "tp"),
        P("sp", "tp"),
        P("sp", "tp"),
        P("sp", "tp"),
        P("sp", "tp"),
        P("sp", None),
        P("sp", None),
        P("tp", None),
        P("tp", None),
    )
    out_specs = (P("sp", "tp"), P("sp", "tp"), P("sp", "tp"))
    return jax.shard_map(shards, mesh=mesh, in_specs=in_specs, out_specs=out_specs, check_vma=False)
```

profile of v0, /device:TPU:0, one launch (start us, length us, event | category | flops | bytes accessed | tf_op | source)
XLA Modules:
  0.0 304.8 jit_solution(12702711185217964215)
XLA Ops:
  7.3 1.8 pad_maximum_fusion.1
  10.6 45.5 %all_gather.7 = f32[2,2048,4]{1,2,0:T(4,128)} all-gather(f32[2,128,4]{1,2,0:T(4,128)S(1)} %pad_maximum_fusion.2), channel_id=1, replica_groups=mesh['sp'=16,'tp'=2] {'sp'}, dimensions={1}, use_global_device_ids=true | all-gather | bytes 69632 | tf_op jit(solution)/shard_map/all_gather | solution.py:44
  57.0 32.9 %all-gather.2.cloned.1.call-done = bf16[2,2048,512]{2,1,0:T(8,128)(2,1)} async-done(((bf16[2,128,512]{2,1,0:T(8,128)(2,1)}), bf16[2,2048,512]{2,1,0:T(8,128)(2,1)}) %all-gather.2.cloned.1.call-update) | async-done | bytes 4194320 | tf_op jit(solution)/shard_map/all_gather | solution.py:56
  89.9 2.5 broadcast_in_dim.3.clone
  92.5 45.4 %while.19 = (s32[]{:T(128)}, f32[2048,512]{1,0:T(8,128)}, f32[512,256]{1,0:T(8,128)S(1)}, f32[512,256]{1,0:T(8,128)S(1)}, bf16[2,2048,512]{2,1,0:T(8,128)(2,1)},...) while((s32[]{:T(128)}, f32[2048,512]{1,0:T(8,128)}, ...), condition=%wide.region_2.3_spmd, body=%wide.region_1.2_spmd.sunk | while | flops 2705326080 | bytes 81904344 | solution.py:97
  93.5 1.4 fusion.137
  95.0 1.8 multiply_convert_fusion.8
  107.5 1.6 pad_maximum_fusion.4
  109.1 2.9 copy.33
  112.1 3.1 %constant_dynamic-update-slice_fusion.2 = f32[2048,512]{1,0:T(8,128)} fusion(f32[2048,512]{1,0:T(8,128)} %get-tuple-element.680, f32[1024,512]{1,0:T(8,128)} %copy.33, s32[]{:T(128)S(6)} %select_n.90), kind=kLoop, calls=%fused_computation.64.clone.1 | loop fusion | bytes 4194308 | tf_op jit(solution)/shard_map/while/body/eval_jaxpr/dynamic_update_slice | solution.py:92
  116.2 1.4 fusion.137
  117.6 1.8 multiply_convert_fusion.8
  130.2 1.6 pad_maximum_fusion.4
  131.8 2.9 copy.33
  134.8 3.1 %constant_dynamic-update-slice_fusion.2 = f32[2048,512]{1,0:T(8,128)} fusion(f32[2048,512]{1,0:T(8,128)} %get-tuple-element.680, f32[1024,512]{1,0:T(8,128)} %copy.33, s32[]{:T(128)S(6)} %select_n.90), kind=kLoop, calls=%fused_computation.64.clone.1 | loop fusion | bytes 4194308 | tf_op jit(solution)/shard_map/while/body/eval_jaxpr/dynamic_update_slice | solution.py:92
  137.9 5.4 %copy.24 = f32[16,128,512]{1,2,0:T(8,128)} copy(f32[16,128,512]{2,1,0:T(8,128)} %bitcast.159) | data formatting | bytes 8388608 | tf_op jit(solution)/shard_map/reshape | solution.py:98
  143.2 4.5 %all-to-all-start = ((f32[16,128,512]{1,2,0:T(8,128)}), f32[16,128,512]{1,2,0:T(8,128)}, u32[]{:S(2)}, u32[]{:S(2)}) async-start(f32[16,128,512]{1,2,0:T(8,128)} %copy.24), calls=%async_computation | async-start | bytes 8388608 | tf_op jit(solution)/shard_map/all_to_all | solution.py:99
  149.5 21.9 %all-reduce.3.cloned.1.call-done = (bf16[512,256]{1,0:T(8,128)(2,1)}, bf16[512,256]{1,0:T(8,128)(2,1)}) async-done(((bf16[512,256]{1,0:T(8,128)(2,1)}, bf16[512,256]{1,0:T(8,128)(2,1)}), (bf16[512,256]{1,0:T(8,128)(2,1)}, bf16[512,256]{1,0:T(8,128)(2,1)})) %all-reduce.3.cloned.1.call-update) | async-done | bytes 524304 | tf_op jit(solution)/shard_map/psum | solution.py:102
  171.4 3.1 %convolution_multiply_fusion = f32[256,2048]{1,0:T(8,128)} fusion(bf16[512,256]{1,0:T(8,128)(2,1)} %get-tuple-element.504, bf16[512,2048]{1,0:T(8,128)(2,1)S(1)} %copy-done), kind=kOutput, calls=%fused_computation.70 | convolution fusion | flops 537395200 | bytes 4456448 | tf_op jit(solution)/shard_map/dot_general | solution.py:14
  174.5 1.2 copy-done.10
  177.0 2.8 convolution_add_fusion.8
  179.8 56.6 %all-to-all-done = f32[16,128,512]{1,2,0:T(8,128)} async-done(((f32[16,128,512]{1,2,0:T(8,128)}), f32[16,128,512]{1,2,0:T(8,128)}, u32[]{:S(2)}, u32[]{:S(2)}) %all-to-all-start) | async-done | bytes 4194336 | tf_op jit(solution)/shard_map/all_to_all | solution.py:99
  236.4 2.4 reduce_sum.19
  239.6 58.6 %reduce-scatter.2.cloned.1.call-done = f32[16,2048]{1,0:T(8,128)} async-done(((f32[256,2048]{1,0:T(8,128)}), f32[16,2048]{1,0:T(8,128)}) %reduce-scatter.2.cloned.1.call-update) | async-done | bytes 131088 | tf_op jit(solution)/shard_map/reduce_scatter | solution.py:109
  (95 shorter events, 29.7 us)
Async XLA Ops:
  7.2 164.3 %copy-start = (bf16[512,2048]{1,0:T(8,128)(2,1)S(1)}, bf16[512,2048]{1,0:T(8,128)(2,1)}, u32[]{:S(2)}) copy-start(bf16[512,2048]{1,0:T(8,128)(2,1)} %param.15) | copy-start | bytes 6291460
  7.2 3.4 %copy-start.13 = (f32[128,4]{0,1:T(4,128)S(1)}, f32[128,4]{0,1:T(4,128)}, u32[]{:S(2)}) copy-start(f32[128,4]{0,1:T(4,128)} %param.14) | copy-start | bytes 6148
  7.2 48.9 %copy-start.8 = (bf16[512,256]{1,0:T(8,128)(2,1)S(1)}, bf16[512,256]{1,0:T(8,128)(2,1)}, u32[]{:S(2)}) copy-start(bf16[512,256]{1,0:T(8,128)(2,1)} %param.17) | copy-start | bytes 786436
  7.2 48.9 %copy-start.9 = (bf16[512,256]{1,0:T(8,128)(2,1)S(1)}, bf16[512,256]{1,0:T(8,128)(2,1)}, u32[]{:S(2)}) copy-start(bf16[512,256]{1,0:T(8,128)(2,1)} %param.16) | copy-start | bytes 786436
  7.2 82.6 %all-gather.2.cloned.1.call-start = ((), (), s32[]{:S(2)}) async-start(), calls=%async_computation.2 | async-start | bytes 4456448 | tf_op jit(solution)/shard_map/all_gather | solution.py:56
  92.5 2.5 copy-start.3
  94.9 2.3 copy-start.1
  96.8 1.0 copy-start.5
  98.5 0.9 copy-start.4
  99.4 1.2 copy-start.2
  103.5 0.9 copy-start.6
  115.2 2.5 copy-start.3
  117.6 2.3 copy-start.1
  119.5 1.0 copy-start.5
  121.2 0.9 copy-start.4
  122.1 1.2 copy-start.2
  126.2 0.9 copy-start.6
  143.2 93.1 %all-to-all-start = ((f32[16,128,512]{1,2,0:T(8,128)}), f32[16,128,512]{1,2,0:T(8,128)}, u32[]{:S(2)}, u32[]{:S(2)}) async-start(f32[16,128,512]{1,2,0:T(8,128)} %copy.24), calls=%async_computation | async-start | bytes 8388608 | tf_op jit(solution)/shard_map/all_to_all | solution.py:99
  147.8 23.7 %all-reduce.3.cloned.1.call-start = ((), (), s32[]{:S(2)}) async-start(), calls=%async_computation.4 | async-start | bytes 1048576 | tf_op jit(solution)/shard_map/psum | solution.py:102
  149.3 148.9 %reduce-scatter.2.cloned.1.call-start = ((), (), s32[]{:S(2)}) async-start(), calls=%async_computation.3 | async-start | bytes 2228224 | tf_op jit(solution)/shard_map/reduce_scatter | solution.py:109
  174.5 1.2 copy-start.10
  174.5 1.3 copy-start.11
  175.8 1.2 copy-start.7
  175.8 1.3 copy-start.12
Sparse Core Ops, SparseCore 0:
  11.3 78.4 all-gather.1
  151.5 19.8 all-reduce.2
  174.7 123.5 reduce-scatter.1
where the time goes:
time: 305 us
  waiting for transfers between devices  170 us (56%)
  blocking collectives  45.5 us (15%)
  matrix products  33.8 us (11%)
  local copies, waits for them, and re-layouts  26.2 us (9%)
  between operations  13.9 us (5%)
  other arithmetic  10.2 us (3%)
  starting transfers between devices  4.85 us (2%)
    reduce_scatter x1, waiting for transfers between devices, shards(): lax.psum_scatter(contract_rows(key_half, source) * weight_scale, 'sp', sc...  58.6 us
    all_to_all x1, waiting for transfers between devices, shards(): lax.all_to_all(stacked, 'sp', split_axis=0, concat_axis=0, tiled=True)  56.6 us
    all_gather x1, blocking collectives, shards(): whole_stats = lax.all_gather(row_stats, 'sp', axis=1, tiled=True)  45.5 us
    all_gather x1, waiting for transfers between devices, shards(): whole_blocks = lax.all_gather(row_blocks, 'sp', axis=1, tiled=True)  32.9 us
    psum x1, waiting for transfers between devices, shards(): lax.psum(key_acc.astype(jnp.bfloat16), 'tp').astype(jnp.float32)  21.9 us
    dot_general x18, matrix products, contract_cols(): lax.dot_general(left, right, (((1,), (1,)), ((), ())), preferred_element_...  16.7 us
    dot_general x17, matrix products, contract_rows(): lax.dot_general(left, right, (((0,), (0,)), ((), ())), preferred_element_...  13.2 us
    dynamic_update_slice x4, local copies, waits for them, and re-layouts, step(): lax.dynamic_update_slice_in_dim(query_buf, jnp.concatenate(parts, axis=1)...  12 us
  transfers between devices with their start and end apart: 4, of which 4 were waited for; matrix products, arithmetic and copies ran while one was open for 4% of the time, Pallas kernels for 0%

commit v1 on v0

v1 whole, which is shorter than its diff:
```python
import functools
import math

import jax
import jax.numpy as jnp
from jax import lax
from jax.experimental import pallas as pl
from jax.experimental.pallas import tpu as pltpu
from jax.sharding import PartitionSpec as P

HEADS = 8
KV_HEADS = 2
HEAD_DIM = 128
LOG2E = 1.0 / math.log(2.0)
MESH = pl.DeviceIdType.MESH
F32 = jnp.float32
BF16 = jnp.bfloat16


def dot_nt(left, right, precision=None):
    return lax.dot_general(
        left, right, (((1,), (1,)), ((), ())), preferred_element_type=F32, precision=precision
    )


def dot_tn(left, right):
    return lax.dot_general(left, right, (((0,), (0,)), ((), ())), preferred_element_type=F32)


def dot_nn(left, right):
    return jnp.dot(left, right, preferred_element_type=F32)


def kernel(
    tgt_n, src_n, tp_n, src_total,
    q_ref, o_ref, d_ref, lse_ref, key_ref, value_ref, source_ref,
    dq_ref, kv_ref, kg_ref,
    qd, stats, kvs, dk, dv, dq_acc, dq_own, dq_out, dq_in, g_out, g_in, tp_own, tp_in,
    src, w_own, w_out, w_in, w2_out, w2_in,
    copy_sem, qd_s, qd_r, st_s, st_r, kv_s, kv_r, dq_s, dq_r, g_s, g_r, tp_s, tp_r,
    w_s, w_r, w2_s, w2_r,
):
    sp = lax.axis_index("sp")
    tp = lax.axis_index("tp")
    me_t, me_s = sp // src_n, sp % src_n
    rows = q_ref.shape[0]
    heads = q_ref.shape[1] // HEAD_DIM
    src_rows = key_ref.shape[0]
    per_key = HEADS // KV_HEADS
    scale = 1.0 / math.sqrt(HEAD_DIM)
    kv_col = pl.multiple_of(tp * heads // per_key * HEAD_DIM, HEAD_DIM)
    t_peers = [lax.rem(me_t + k, tgt_n) for k in range(1, tgt_n)]
    s_peers = [lax.rem(me_s + k, src_n) for k in range(1, src_n)]
    tp_peers = [lax.rem(tp + k, tp_n) for k in range(1, tp_n)]

    def t_dev(t):
        return {"sp": t * src_n + me_s, "tp": tp}

    def s_dev(s):
        return {"sp": me_t * src_n + s, "tp": tp}

    def tp_dev(p):
        return {"sp": sp, "tp": p}

    def remote(source, target, send, recv, device):
        return pltpu.make_async_remote_copy(
            src_ref=source, dst_ref=target, send_sem=send, recv_sem=recv,
            device_id=device, device_id_type=MESH,
        )

    load = pltpu.make_async_copy(source_ref, src, copy_sem)
    load.start()
    barrier = pltpu.get_barrier_semaphore()
    for t in t_peers:
        pl.semaphore_signal(barrier, inc=1, device_id=t_dev(t), device_id_type=MESH)
    for s in s_peers:
        pl.semaphore_signal(barrier, inc=1, device_id=s_dev(s), device_id_type=MESH)
    for p in tp_peers:
        pl.semaphore_signal(barrier, inc=1, device_id=tp_dev(p), device_id_type=MESH)
    pl.semaphore_wait(barrier, tgt_n + src_n + tp_n - 3)

    for t in t_peers:
        for h in range(heads):
            for i, ref in enumerate((q_ref, d_ref)):
                remote(
                    ref.at[:, pl.ds(h * HEAD_DIM, HEAD_DIM)],
                    qd.at[me_t, i, pl.ds(h * rows, rows), :],
                    qd_s.at[t], qd_r.at[me_t], t_dev(t),
                ).start()
    for s in s_peers:
        for i, ref in enumerate((key_ref, value_ref)):
            remote(
                ref.at[:, pl.ds(kv_col, HEAD_DIM)], kvs.at[me_s, i],
                kv_s.at[s], kv_r.at[me_s], s_dev(s),
            ).start()

    ones = jnp.ones((8, HEAD_DIM), F32)
    for h in range(heads):
        cols = pl.ds(h * HEAD_DIM, HEAD_DIM)
        span = pl.ds(h * rows, rows)
        prod = d_ref[:, cols].astype(F32) * o_ref[:, cols].astype(F32)
        delta = dot_nt(ones, prod, lax.Precision.HIGHEST)
        stats[me_t, 0:1, span] = lse_ref[h : h + 1, :] * LOG2E
        stats[me_t, 1:2, span] = delta[0:1, :]
        qd[me_t, 0, span, :] = q_ref[:, cols]
        qd[me_t, 1, span, :] = d_ref[:, cols]
    kvs[me_s, 0] = key_ref[:, pl.ds(kv_col, HEAD_DIM)]
    kvs[me_s, 1] = value_ref[:, pl.ds(kv_col, HEAD_DIM)]
    dk[...] = jnp.zeros_like(dk)
    dv[...] = jnp.zeros_like(dv)
    for t in t_peers:
        remote(stats.at[me_t], stats.at[me_t], st_s.at[t], st_r.at[me_t], t_dev(t)).start()

    def tile(t, s):
        q, d = qd[t, 0], qd[t, 1]
        k, v = kvs[s, 0], kvs[s, 1]
        scores = dot_nt(k, q)
        probs = jnp.exp2(scores * (scale * LOG2E) - stats[t, 0:1, :])
        dprobs = dot_nt(v, d)
        dscores = (probs * (dprobs - stats[t, 1:2, :])).astype(BF16)
        dv[s] += dot_nn(probs.astype(BF16), d)
        dk[s] += dot_nn(dscores, q)
        dq_acc[...] += dot_tn(dscores, k)

    def send_dq(t):
        dq_out[t] = (dq_acc[...] * scale).astype(BF16)
        remote(dq_out.at[t], dq_in.at[me_t], dq_s.at[t], dq_r.at[me_t], t_dev(t)).start()

    def send_kv(s):
        g_out[s, 0] = (dk[s] * scale).astype(BF16)
        g_out[s, 1] = dv[s].astype(BF16)
        remote(g_out.at[s], g_in.at[me_s], g_s.at[s], g_r.at[me_s], s_dev(s)).start()

    dq_acc[...] = jnp.zeros_like(dq_acc)
    tile(me_t, me_s)
    for s in s_peers:
        remote(kvs.at[s], kvs.at[s], kv_s.at[s], kv_r.at[s], s_dev(s)).wait_recv()
        tile(me_t, s)
    dq_own[...] = dq_acc[...] * scale
    for n, t in enumerate(t_peers):
        remote(qd.at[t], qd.at[t], qd_s.at[t], qd_r.at[t], t_dev(t)).wait_recv()
        remote(stats.at[t], stats.at[t], st_s.at[t], st_r.at[t], t_dev(t)).wait_recv()
        dq_acc[...] = jnp.zeros_like(dq_acc)
        if n < tgt_n - 2:

            def body(s, carry, t=t):
                tile(t, s)
                return carry

            lax.fori_loop(0, src_n, body, 0)
        else:
            for s in s_peers:
                tile(t, s)
                send_kv(s)
            tile(t, me_s)
        send_dq(t)

    dk_total = dk[me_s] * scale
    dv_total = dv[me_s]
    for s in s_peers:
        remote(g_in.at[s], g_in.at[s], g_s.at[s], g_r.at[s], s_dev(s)).wait_recv()
        dk_total += g_in[s, 0].astype(F32)
        dv_total += g_in[s, 1].astype(F32)
    tp_own[0] = dk_total.astype(BF16)
    tp_own[1] = dv_total.astype(BF16)
    for p in tp_peers:
        remote(tp_own, tp_in.at[tp], tp_s.at[p], tp_r.at[tp], tp_dev(p)).start()
    tp_in[tp] = tp_own[...]
    for p in tp_peers:
        remote(tp_in.at[p], tp_in.at[p], tp_s.at[p], tp_r.at[p], tp_dev(p)).wait_recv()
    for i in range(2):
        for g in range(KV_HEADS):
            owners = [p for p in range(tp_n) if p * heads // per_key == g]
            half = tp_in[owners[0], i]
            if len(owners) > 1:
                total = half.astype(F32)
                for p in owners[1:]:
                    total += tp_in[p, i].astype(F32)
                half = total.astype(BF16)
            kv_ref[:, pl.ds((i * KV_HEADS + g) * HEAD_DIM, HEAD_DIM)] = half

    load.wait()
    part = w_own.shape[1]
    key_half = kv_ref[:, 0 : KV_HEADS * HEAD_DIM]
    w_scale = 1.0 / math.sqrt(src_total)
    partial = dot_tn(key_half, src[...]) * w_scale
    for t in range(tgt_n):
        for s in range(src_n):
            low = (t * src_n + s) * part
            w_out[s, t] = partial[low : low + part].astype(BF16)
    for s in s_peers:
        remote(w_out.at[s], w_in.at[me_s], w_s.at[s], w_r.at[me_s], s_dev(s)).start()

    dq_total = dq_own[...]
    for t in t_peers:
        remote(dq_in.at[t], dq_in.at[t], dq_s.at[t], dq_r.at[t], t_dev(t)).wait_recv()
        dq_total += dq_in[t].astype(F32)
    for h in range(heads):
        dq_ref[:, h * HEAD_DIM : (h + 1) * HEAD_DIM] = dq_total[h * rows : (h + 1) * rows]

    w_total = w_out[me_s].astype(F32)
    for s in s_peers:
        remote(w_in.at[s], w_in.at[s], w_s.at[s], w_r.at[s], s_dev(s)).wait_recv()
        w_total += w_in[s].astype(F32)
    w_own[...] = w_total
    w2_out[...] = w_total.astype(BF16)
    for t in t_peers:
        remote(w2_out.at[t], w2_in.at[me_t], w2_s.at[t], w2_r.at[me_t], t_dev(t)).start()
    kg_total = w_own[me_t]
    for t in t_peers:
        remote(w2_in.at[t], w2_in.at[t], w2_s.at[t], w2_r.at[t], t_dev(t)).wait_recv()
        kg_total += w2_in[t].astype(F32)
    kg_ref[...] = kg_total

    for t in t_peers:
        remote(qd.at[t], qd.at[t], qd_s.at[t], qd_r.at[t], t_dev(t)).wait_send()
        remote(stats.at[t], stats.at[t], st_s.at[t], st_r.at[t], t_dev(t)).wait_send()
        remote(dq_out.at[t], dq_in.at[t], dq_s.at[t], dq_r.at[t], t_dev(t)).wait_send()
        remote(w2_out.at[t], w2_in.at[t], w2_s.at[t], w2_r.at[t], t_dev(t)).wait_send()
    for s in s_peers:
        remote(kvs.at[s], kvs.at[s], kv_s.at[s], kv_r.at[s], s_dev(s)).wait_send()
        remote(g_out.at[s], g_in.at[s], g_s.at[s], g_r.at[s], s_dev(s)).wait_send()
        remote(w_out.at[s], w_in.at[s], w_s.at[s], w_r.at[s], s_dev(s)).wait_send()
    for p in tp_peers:
        remote(tp_own, tp_in.at[p], tp_s.at[p], tp_r.at[p], tp_dev(p)).wait_send()


def shards(
    tgt_n, src_n, tp_n,
    queries, attn_out, out_grad, row_lse, source, saved_keys, saved_values, key_weight, value_weight
):
    heads = row_lse.shape[1]
    rows, width = queries.shape
    src_rows, columns = source.shape
    kv_width = KV_HEADS * HEAD_DIM
    sp_n = tgt_n * src_n
    part = kv_width // sp_n
    stacked = heads * rows
    dma = pltpu.SemaphoreType.DMA
    vmem = pl.BlockSpec(memory_space=pltpu.VMEM)
    scratch = [
        pltpu.VMEM((tgt_n, 2, stacked, HEAD_DIM), BF16),
        pltpu.VMEM((tgt_n, 8, stacked), F32),
        pltpu.VMEM((src_n, 2, src_rows, HEAD_DIM), BF16),
        pltpu.VMEM((src_n, src_rows, HEAD_DIM), F32),
        pltpu.VMEM((src_n, src_rows, HEAD_DIM), F32),
        pltpu.VMEM((stacked, HEAD_DIM), F32),
        pltpu.VMEM((stacked, HEAD_DIM), F32),
        pltpu.VMEM((tgt_n, stacked, HEAD_DIM), BF16),
        pltpu.VMEM((tgt_n, stacked, HEAD_DIM), BF16),
        pltpu.VMEM((src_n, 2, src_rows, HEAD_DIM), BF16),
        pltpu.VMEM((src_n, 2, src_rows, HEAD_DIM), BF16),
        pltpu.VMEM((2, src_rows, HEAD_DIM), BF16),
        pltpu.VMEM((tp_n, 2, src_rows, HEAD_DIM), BF16),
        pltpu.VMEM((src_rows, columns), BF16),
        pltpu.VMEM((tgt_n, part, columns), F32),
        pltpu.VMEM((src_n, tgt_n, part, columns), BF16),
        pltpu.VMEM((src_n, tgt_n, part, columns), BF16),
        pltpu.VMEM((tgt_n, part, columns), BF16),
        pltpu.VMEM((tgt_n, part, columns), BF16),
        dma,
    ]
    for count in (tgt_n, tgt_n, src_n, tgt_n, src_n, tp_n, src_n, tgt_n):
        scratch += [dma((count,)), dma((count,))]
    query_grad, kv_half, key_grad = pl.pallas_call(
        functools.partial(kernel, tgt_n, src_n, tp_n, src_rows * sp_n),
        out_shape=(
            jax.ShapeDtypeStruct((rows, width), F32),
            jax.ShapeDtypeStruct((src_rows, 2 * kv_width), BF16),
            jax.ShapeDtypeStruct((part, columns), F32),
        ),
        in_specs=[vmem] * 6 + [pl.BlockSpec(memory_space=pl.ANY)],
        out_specs=(vmem, vmem, vmem),
        scratch_shapes=scratch,
        compiler_params=pltpu.CompilerParams(
            collective_id=0, has_side_effects=True, vmem_limit_bytes=60 * 2**20
        ),
        name="attention_grads",
    )(queries, attn_out, out_grad, row_lse.T, saved_keys, saved_values, source)
    source_grad = dot_nt(kv_half[:, :kv_width], key_weight) + dot_nt(
        kv_half[:, kv_width:], value_weight
    )
    return (query_grad, source_grad, key_grad)


def solution(mesh):
    sp_n, tp_n = mesh.shape["sp"], mesh.shape["tp"]
    src_n = 2 ** (int(math.log2(sp_n)) // 2)
    in_specs = (
        P("sp", "tp"),
        P("sp", "tp"),
        P("sp", "tp"),
        P("sp", "tp"),
        P("sp", "tp"),
        P("sp", None),
        P("sp", None),
        P("tp", None),
        P("tp", None),
    )
    out_specs = (P("sp", "tp"), P("sp", "tp"), P("sp", "tp"))
    return jax.shard_map(
        functools.partial(shards, sp_n // src_n, src_n, tp_n),
        mesh=mesh, in_specs=in_specs, out_specs=out_specs, check_vma=False,
    )
```

time: 305 us -> 79.8 us (0.26)
  waiting for transfers between devices: 170 us -> 0 us
  Pallas kernels: 0 us -> 73 us
  blocking collectives: 45.5 us -> 0 us
  matrix products: 33.8 us -> 4.52 us
  local copies, waits for them, and re-layouts: 26.2 us -> 1.38 us
  between operations: 13.9 us -> 0.71 us
  other arithmetic: 10.2 us -> 0 us
  starting transfers between devices: 4.85 us -> 0 us
    pallas_call x0 -> x1, Pallas kernels: none -> 73 us  [shards(): pl.pallas_call(functools.partial(kernel, tgt_n, src_n, tp_n, src_rows * s...]
    reduce_scatter x1 -> x0, waiting for transfers between devices: 58.6 us -> none  [shards(): lax.psum_scatter(contract_rows(key_half, source) * weight_scale, 'sp', sc...]
    all_to_all x1 -> x0, waiting for transfers between devices: 56.6 us -> none  [shards(): lax.all_to_all(stacked, 'sp', split_axis=0, concat_axis=0, tiled=True)]
    all_gather x1 -> x0, blocking collectives: 45.5 us -> none  [shards(): whole_stats = lax.all_gather(row_stats, 'sp', axis=1, tiled=True)]
    all_gather x1 -> x0, waiting for transfers between devices: 32.9 us -> none  [shards(): whole_blocks = lax.all_gather(row_blocks, 'sp', axis=1, tiled=True)]
    dot_general x43 -> x2, matrix products: 33.8 us -> 4.52 us  [dot_nt(): lax.dot_general(left, right, (((1,), (1,)), ((), ())), preferred_element_...]
    psum x1 -> x0, waiting for transfers between devices: 21.9 us -> none  [shards(): lax.psum(key_acc.astype(jnp.bfloat16), 'tp').astype(jnp.float32)]
    dynamic_update_slice x4 -> x0, local copies, waits for them, and re-layouts: 12 us -> none  [step(): lax.dynamic_update_slice_in_dim(query_buf, jnp.concatenate(parts, axis=1)...]
  transfers between devices with their start and end apart: 4 -> 0, of which waited for: 4 -> 0; matrix products, arithmetic and copies ran while one was open for 4% -> 0% of each run, Pallas kernels for 0% -> 0%
where the time goes in v1:
time: 79.8 us; the launch traced here: 79.6 us
  Pallas kernels  73 us (91%)
  matrix products  4.52 us (6%)
  local copies, waits for them, and re-layouts  1.38 us (2%)
    pallas_call x1, Pallas kernels, shards(): pl.pallas_call(functools.partial(kernel, tgt_n, src_n, tp_n, src_rows * s...  73 us
    dot_general x2, matrix products, dot_nt(): lax.dot_general(left, right, (((1,), (1,)), ((), ())), preferred_element_...  4.52 us

profile of v1, /device:TPU:0, one launch (start us, length us, event | category | flops | bytes accessed | tf_op | source)
XLA Modules:
  0.0 79.6 jit_solution(5563199093546283206)
XLA Ops:
  0.6 0.0 copy-start
  0.6 0.0 copy-start.1
  0.7 73.0 %attention_grads.1 = (f32[128,512]{1,0:T(8,128)}, bf16[512,512]{1,0:T(8,128)(2,1)}, f32[16,2048]{1,0:T(8,128)}) custom-call(bf16[128,512]{1,0:T(8,128)(2,1)} %q_ref.1, bf16[128,512]{1,0:T(8,128)(2,1)} %o_ref.1, bf16[128,512]{1,0:T(8,128)(2,1)} %d_ref.1, f32[4,128]{1,0:T(4,128)} %bitcast.3, bf16[512,256]{1,0:T(8,128)(2,1)} %key_ref.1, ...), custom_call_target="tpu_custom_call" | custom-call | tf_op jit(solution)/shard_map/attention_grads/pallas_call | solution.py:265
  73.6 0.0 copy-start.2
  73.7 0.0 copy-done
  73.7 1.7 %fusion.1 = f32[512,2048]{1,0:T(8,128)S(1)} fusion(bf16[2048,256]{1,0:T(8,128)(2,1)S(1)} %copy-done, bf16[512,512]{1,0:T(8,128)(2,1)} %get-tuple-element.7), kind=kOutput, calls=%fused_computation.2 | convolution fusion | flops 536870912 | bytes 5505024 | tf_op jit(solution)/shard_map/dot_general | solution.py:21
  75.4 0.0 copy-done.1
  75.4 0.0 copy-done.2
  75.4 0.0 copy-start.3
  75.4 0.0 copy-start.4
  75.5 2.8 %convolution_add_fusion = f32[512,2048]{1,0:T(8,128)} fusion(f32[512,2048]{1,0:T(8,128)S(1)} %fusion.1, bf16[2048,256]{1,0:T(8,128)(2,1)S(1)} %copy-done.1, bf16[512,512]{1,0:T(8,128)(2,1)S(1)} %copy-done.2), kind=kOutput, calls=%fused_computation | convolution fusion | flops 537919488 | bytes 9699328 | tf_op jit(solution)/shard_map/dot_general | solution.py:21
  78.2 0.0 copy-done.3
  78.2 0.7 copy.14
  78.9 0.0 copy-done.4
  78.9 0.7 copy.15
Async XLA Ops:
  0.6 73.0 %copy-start = (bf16[2048,256]{1,0:T(8,128)(2,1)S(1)}, bf16[2048,256]{1,0:T(8,128)(2,1)}, u32[]{:S(2)}) copy-start(bf16[2048,256]{1,0:T(8,128)(2,1)} %param.16) | copy-start | bytes 3145732
  0.6 74.8 %copy-start.1 = (bf16[2048,256]{1,0:T(8,128)(2,1)S(1)}, bf16[2048,256]{1,0:T(8,128)(2,1)}, u32[]{:S(2)}) copy-start(bf16[2048,256]{1,0:T(8,128)(2,1)} %param.17) | copy-start | bytes 3145732
  73.6 1.8 %copy-start.2 = (bf16[512,512]{1,0:T(8,128)(2,1)S(1)}, bf16[512,512]{1,0:T(8,128)(2,1)}, u32[]{:S(2)}) copy-start(bf16[512,512]{1,0:T(8,128)(2,1)} %get-tuple-element.7) | copy-start | bytes 1572868
  75.4 2.8 %copy-start.3 = (f32[128,512]{1,0:T(8,128)S(1)}, f32[128,512]{1,0:T(8,128)}, u32[]{:S(2)}) copy-start(f32[128,512]{1,0:T(8,128)} %get-tuple-element.12) | copy-start | bytes 786436
  75.4 3.5 %copy-start.4 = (f32[16,2048]{1,0:T(8,128)S(1)}, f32[16,2048]{1,0:T(8,128)}, u32[]{:S(2)}) copy-start(f32[16,2048]{1,0:T(8,128)} %get-tuple-element.14) | copy-start | bytes 393220

commit v2 on v1

v2 whole, which is shorter than its diff:
```python
import functools
import math

import jax
import jax.numpy as jnp
from jax import lax
from jax.experimental import pallas as pl
from jax.experimental.pallas import tpu as pltpu
from jax.sharding import PartitionSpec as P

HEADS = 8
KV_HEADS = 2
HEAD_DIM = 128
LOG2E = 1.0 / math.log(2.0)
MESH = pl.DeviceIdType.MESH
F32 = jnp.float32
BF16 = jnp.bfloat16


def dot_nt(left, right, precision=None):
    return lax.dot_general(
        left, right, (((1,), (1,)), ((), ())), preferred_element_type=F32, precision=precision
    )


def dot_tn(left, right):
    return lax.dot_general(left, right, (((0,), (0,)), ((), ())), preferred_element_type=F32)


def dot_nn(left, right):
    return jnp.dot(left, right, preferred_element_type=F32)


def kernel(
    tgt_n, src_n, key_n, tp_n, src_total,
    q_ref, o_ref, d_ref, lse_ref, key_ref, value_ref, source_ref,
    dq_ref, kv_ref, kg_ref,
    qd, stats, kvs, dk, dv, dq_acc, dq_out, dq_in, g_out, g_in, tp_own, tp_in,
    src, a_out, a_in, a2_own, a2_out, a2_in, b_out, b_in, b2_own, b2_out, b2_in,
    copy_sem, qd_s, qd_r, rq_s, st_s, st_r, kv_s, kv_r, rkv_s, dq_s, dq_r, g_s, g_r, tp_s, tp_r,
    a_s, a_r, a2_s, a2_r, b_s, b_r, b2_s, b2_r,
):
    sp = lax.axis_index("sp")
    tp = lax.axis_index("tp")
    sp_n = tgt_n * src_n
    t_hi, t_lo = sp // (2 * src_n), sp % 2
    me_t = t_hi * 2 + t_lo
    me_s = (sp // 2) % src_n
    s_hi, s_lo = me_s // 2, me_s % 2
    near_t, near_s = t_hi * 2 + 1 - t_lo, s_hi * 2 + 1 - s_lo
    t_his = [lax.rem(t_hi + k, tgt_n // 2) for k in range(1, tgt_n // 2)]
    s_his = [lax.rem(s_hi + k, src_n // 2) for k in range(1, src_n // 2)]
    far_t = [hi * 2 + t_lo for hi in t_his]
    diag_t = [hi * 2 + 1 - t_lo for hi in t_his]
    far_s = [hi * 2 + s_lo for hi in s_his]
    diag_s = [hi * 2 + 1 - s_lo for hi in s_his]
    t_peers = far_t + [near_t] + diag_t
    s_peers = far_s + [near_s] + diag_s
    key_m = sp_n // key_n
    me_o, me_i = sp // key_n, sp % key_n
    o_peers = [lax.rem(me_o + k, key_m) for k in range(1, key_m)]
    i_peers = [lax.rem(me_i + k, key_n) for k in range(1, key_n)]
    tp_peers = [lax.rem(tp + k, tp_n) for k in range(1, tp_n)]
    rows = q_ref.shape[0]
    heads = q_ref.shape[1] // HEAD_DIM
    chunks = qd.shape[1]
    per_chunk = heads // chunks
    src_rows = key_ref.shape[0]
    per_key = HEADS // KV_HEADS
    scale = 1.0 / math.sqrt(HEAD_DIM)
    kv_col = pl.multiple_of(tp * heads // per_key * HEAD_DIM, HEAD_DIM)

    def t_dev(t):
        return {"sp": t // 2 * (2 * src_n) + me_s * 2 + t % 2, "tp": tp}

    def s_dev(s):
        return {"sp": t_hi * (2 * src_n) + s * 2 + t_lo, "tp": tp}

    def o_dev(o):
        return {"sp": o * key_n + me_i, "tp": tp}

    def i_dev(i):
        return {"sp": me_o * key_n + i, "tp": tp}

    def tp_dev(p):
        return {"sp": sp, "tp": p}

    def remote(source, target, send, recv, device):
        return pltpu.make_async_remote_copy(
            src_ref=source, dst_ref=target, send_sem=send, recv_sem=recv,
            device_id=device, device_id_type=MESH,
        )

    load = pltpu.make_async_copy(source_ref, src, copy_sem)
    load.start()
    barrier = pltpu.get_barrier_semaphore()
    for k in range(1, sp_n):
        pl.semaphore_signal(
            barrier, inc=1, device_id={"sp": lax.rem(sp + k, sp_n), "tp": tp}, device_id_type=MESH
        )
    for p in tp_peers:
        pl.semaphore_signal(barrier, inc=1, device_id=tp_dev(p), device_id_type=MESH)
    pl.semaphore_wait(barrier, sp_n + tp_n - 2)

    def send_q(t):
        for c in range(chunks):
            for h in range(per_chunk):
                for i, ref in enumerate((q_ref, d_ref)):
                    remote(
                        ref.at[:, pl.ds((c * per_chunk + h) * HEAD_DIM, HEAD_DIM)],
                        qd.at[me_t, c, i, pl.ds(h * rows, rows), :],
                        qd_s.at[t, c], qd_r.at[me_t, c], t_dev(t),
                    ).start()

    for s in far_s + [near_s]:
        for i, ref in enumerate((key_ref, value_ref)):
            remote(
                ref.at[:, pl.ds(kv_col, HEAD_DIM)], kvs.at[me_s, i],
                kv_s.at[s], kv_r.at[me_s], s_dev(s),
            ).start()
    for t in far_t + [near_t]:
        send_q(t)

    ones = jnp.ones((8, HEAD_DIM), F32)
    for h in range(heads):
        cols = pl.ds(h * HEAD_DIM, HEAD_DIM)
        c, span = h // per_chunk, pl.ds(h % per_chunk * rows, rows)
        prod = d_ref[:, cols].astype(F32) * o_ref[:, cols].astype(F32)
        delta = dot_nt(ones, prod, lax.Precision.HIGHEST)
        stats[me_t, c, 0:1, span] = lse_ref[h : h + 1, :] * LOG2E
        stats[me_t, c, 1:2, span] = delta[0:1, :]
        qd[me_t, c, 0, span, :] = q_ref[:, cols]
        qd[me_t, c, 1, span, :] = d_ref[:, cols]
    kvs[me_s, 0] = key_ref[:, pl.ds(kv_col, HEAD_DIM)]
    kvs[me_s, 1] = value_ref[:, pl.ds(kv_col, HEAD_DIM)]
    dk[...] = jnp.zeros_like(dk)
    dv[...] = jnp.zeros_like(dv)
    dq_acc[...] = jnp.zeros_like(dq_acc)
    for t in t_peers:
        remote(stats.at[me_t], stats.at[me_t], st_s.at[t], st_r.at[me_t], t_dev(t)).start()

    def tile(t, s):
        def body(c, carry):
            q, d = qd[t, c, 0], qd[t, c, 1]
            k, v = kvs[s, 0], kvs[s, 1]
            scores = dot_nt(k, q)
            probs = jnp.exp2(scores * (scale * LOG2E) - stats[t, c, 0:1, :])
            dprobs = dot_nt(v, d)
            dscores = (probs * (dprobs - stats[t, c, 1:2, :])).astype(BF16)
            dv[s] += dot_nn(probs.astype(BF16), d)
            dk[s] += dot_nn(dscores, q)
            dq_acc[t, c] += dot_tn(dscores, k)
            return carry

        lax.fori_loop(0, chunks, body, 0)

    def got_q(t, c):
        remote(qd.at[t, c], qd.at[t, c], qd_s.at[t, c], qd_r.at[t, c], t_dev(t)).wait_recv()

    def got_stats(t):
        remote(stats.at[t], stats.at[t], st_s.at[t], st_r.at[t], t_dev(t)).wait_recv()

    def got_kv(s):
        remote(kvs.at[s], kvs.at[s], kv_s.at[s], kv_r.at[s], s_dev(s)).wait_recv()

    def relay_q(t, c):
        return remote(
            qd.at[t, c], qd.at[t, c], rq_s.at[t, c], qd_r.at[t, c], t_dev(near_t)
        )

    def relay_kv(s):
        return remote(kvs.at[s], kvs.at[s], rkv_s.at[s], kv_r.at[s], s_dev(near_s))

    def send_dq(t):
        dq_out[t] = (dq_acc[t] * scale).astype(BF16)
        remote(dq_out.at[t], dq_in.at[me_t], dq_s.at[t], dq_r.at[me_t], t_dev(t)).start()

    def send_g(s, i):
        g_out[s, i] = dv[s].astype(BF16) if i else (dk[s] * scale).astype(BF16)
        remote(
            g_out.at[s, i], g_in.at[me_s, i], g_s.at[s, i], g_r.at[me_s, i], s_dev(s)
        ).start()

    tile(me_t, me_s)
    for s in far_s:
        got_kv(s)
        relay_kv(s).start()
    got_kv(near_s)
    tile(me_t, near_s)
    for c in range(chunks):
        for t in far_t:
            got_q(t, c)
            relay_q(t, c).start()
        if c == 0:
            for s in far_s:
                tile(me_t, s)
            for c2 in range(chunks):
                got_q(near_t, c2)
            got_stats(near_t)
    for s in [me_s, near_s] + far_s:
        tile(near_t, s)
    for t in far_t:
        got_stats(t)
        for s in [me_s, near_s] + far_s:
            tile(t, s)
    for s in diag_s:
        got_kv(s)
        for t in [near_t] + far_t + [me_t]:
            tile(t, s)
    for t in [near_t] + far_t:
        send_dq(t)
    for n, t in enumerate(diag_t):
        for c in range(chunks):
            got_q(t, c)
        got_stats(t)
        for s in far_s + diag_s + [near_s]:
            tile(t, s)
            if n == len(diag_t) - 1:
                send_g(s, 0)
        if n == len(diag_t) - 1:
            for s in far_s + diag_s + [near_s]:
                send_g(s, 1)
        tile(t, me_s)
        send_dq(t)

    def reduce_g(i):
        total = dv[me_s] if i else dk[me_s] * scale
        for s in s_peers:
            remote(
                g_in.at[s, i], g_in.at[s, i], g_s.at[s, i], g_r.at[s, i], s_dev(s)
            ).wait_recv()
            total += g_in[s, i].astype(F32)
        tp_own[i] = total.astype(BF16)
        for p in tp_peers:
            remote(
                tp_own.at[i], tp_in.at[tp, i], tp_s.at[p, i], tp_r.at[tp, i], tp_dev(p)
            ).start()
        tp_in[tp, i] = tp_own[i]

    def gather_g(i):
        for p in tp_peers:
            remote(
                tp_in.at[p, i], tp_in.at[p, i], tp_s.at[p, i], tp_r.at[p, i], tp_dev(p)
            ).wait_recv()
        for g in range(KV_HEADS):
            owners = [p for p in range(tp_n) if p * heads // per_key == g]
            half = tp_in[owners[0], i]
            if len(owners) > 1:
                total = half.astype(F32)
                for p in owners[1:]:
                    total += tp_in[p, i].astype(F32)
                half = total.astype(BF16)
            kv_ref[:, pl.ds((i * KV_HEADS + g) * HEAD_DIM, HEAD_DIM)] = half

    reduce_g(0)
    load.wait()
    gather_g(0)
    part = a2_own.shape[1]
    cut = a2_own.shape[2]
    key_half = kv_ref[:, 0 : KV_HEADS * HEAD_DIM]
    w_scale = 1.0 / math.sqrt(src_total)
    partial = dot_tn(key_half, src[...]) * w_scale
    for o in range(key_m):
        for i in range(key_n):
            low = (o * key_n + i) * part
            block = partial[low : low + part].astype(BF16)
            a_out[i, o] = block[:, :cut]
            b_out[o, i] = block[:, cut:]
    for i in i_peers:
        remote(a_out.at[i], a_in.at[me_i], a_s.at[i], a_r.at[me_i], i_dev(i)).start()
    for o in o_peers:
        remote(b_out.at[o], b_in.at[me_o], b_s.at[o], b_r.at[me_o], o_dev(o)).start()

    reduce_g(1)
    gather_g(1)
    dq_total = dq_acc[me_t] * scale
    for t in t_peers:
        remote(dq_in.at[t], dq_in.at[t], dq_s.at[t], dq_r.at[t], t_dev(t)).wait_recv()
        dq_total += dq_in[t].astype(F32)
    for h in range(heads):
        low = h % per_chunk * rows
        dq_ref[:, h * HEAD_DIM : (h + 1) * HEAD_DIM] = dq_total[h // per_chunk, low : low + rows]

    total = b_out[me_o].astype(F32)
    for o in o_peers:
        remote(b_in.at[o], b_in.at[o], b_s.at[o], b_r.at[o], o_dev(o)).wait_recv()
        total += b_in[o].astype(F32)
    b2_own[...] = total
    b2_out[...] = total.astype(BF16)
    for i in i_peers:
        remote(b2_out.at[i], b2_in.at[me_i], b2_s.at[i], b2_r.at[me_i], i_dev(i)).start()
    total = a_out[me_i].astype(F32)
    for i in i_peers:
        remote(a_in.at[i], a_in.at[i], a_s.at[i], a_r.at[i], i_dev(i)).wait_recv()
        total += a_in[i].astype(F32)
    a2_own[...] = total
    a2_out[...] = total.astype(BF16)
    for o in o_peers:
        remote(a2_out.at[o], a2_in.at[me_o], a2_s.at[o], a2_r.at[me_o], o_dev(o)).start()
    total = b2_own[me_i]
    for i in i_peers:
        remote(b2_in.at[i], b2_in.at[i], b2_s.at[i], b2_r.at[i], i_dev(i)).wait_recv()
        total += b2_in[i].astype(F32)
    kg_ref[:, cut:] = total
    total = a2_own[me_o]
    for o in o_peers:
        remote(a2_in.at[o], a2_in.at[o], a2_s.at[o], a2_r.at[o], o_dev(o)).wait_recv()
        total += a2_in[o].astype(F32)
    kg_ref[:, :cut] = total

    for t in far_t + [near_t]:
        for c in range(chunks):
            remote(qd.at[t, c], qd.at[t, c], qd_s.at[t, c], qd_r.at[t, c], t_dev(t)).wait_send()
    for t in far_t:
        for c in range(chunks):
            relay_q(t, c).wait_send()
    for t in t_peers:
        remote(stats.at[t], stats.at[t], st_s.at[t], st_r.at[t], t_dev(t)).wait_send()
        remote(dq_out.at[t], dq_in.at[t], dq_s.at[t], dq_r.at[t], t_dev(t)).wait_send()
    for s in far_s + [near_s]:
        remote(kvs.at[s], kvs.at[s], kv_s.at[s], kv_r.at[s], s_dev(s)).wait_send()
    for s in far_s:
        relay_kv(s).wait_send()
    for s in s_peers:
        for i in range(2):
            remote(
                g_out.at[s, i], g_in.at[s, i], g_s.at[s, i], g_r.at[s, i], s_dev(s)
            ).wait_send()
    for i in i_peers:
        remote(a_out.at[i], a_in.at[i], a_s.at[i], a_r.at[i], i_dev(i)).wait_send()
        remote(b2_out.at[i], b2_in.at[i], b2_s.at[i], b2_r.at[i], i_dev(i)).wait_send()
    for o in o_peers:
        remote(b_out.at[o], b_in.at[o], b_s.at[o], b_r.at[o], o_dev(o)).wait_send()
        remote(a2_out.at[o], a2_in.at[o], a2_s.at[o], a2_r.at[o], o_dev(o)).wait_send()
    for p in tp_peers:
        for i in range(2):
            remote(
                tp_own.at[i], tp_in.at[p, i], tp_s.at[p, i], tp_r.at[p, i], tp_dev(p)
            ).wait_send()


def shards(
    tgt_n, src_n, tp_n,
    queries, attn_out, out_grad, row_lse, source, saved_keys, saved_values, key_weight, value_weight
):
    heads = row_lse.shape[1]
    rows, width = queries.shape
    src_rows, columns = source.shape
    kv_width = KV_HEADS * HEAD_DIM
    sp_n = tgt_n * src_n
    part = kv_width // sp_n
    key_n, key_m = src_n, tgt_n
    chunks = math.gcd(heads, 2)
    stacked = heads // chunks * rows
    cut = (2 * columns // 3 + 127) // 128 * 128
    rest = columns - cut
    dma = pltpu.SemaphoreType.DMA
    vmem = pl.BlockSpec(memory_space=pltpu.VMEM)
    scratch = [
        pltpu.VMEM((tgt_n, chunks, 2, stacked, HEAD_DIM), BF16),
        pltpu.VMEM((tgt_n, chunks, 8, stacked), F32),
        pltpu.VMEM((src_n, 2, src_rows, HEAD_DIM), BF16),
        pltpu.VMEM((src_n, src_rows, HEAD_DIM), F32),
        pltpu.VMEM((src_n, src_rows, HEAD_DIM), F32),
        pltpu.VMEM((tgt_n, chunks, stacked, HEAD_DIM), F32),
        pltpu.VMEM((tgt_n, chunks, stacked, HEAD_DIM), BF16),
        pltpu.VMEM((tgt_n, chunks, stacked, HEAD_DIM), BF16),
        pltpu.VMEM((src_n, 2, src_rows, HEAD_DIM), BF16),
        pltpu.VMEM((src_n, 2, src_rows, HEAD_DIM), BF16),
        pltpu.VMEM((2, src_rows, HEAD_DIM), BF16),
        pltpu.VMEM((tp_n, 2, src_rows, HEAD_DIM), BF16),
        pltpu.VMEM((src_rows, columns), BF16),
        pltpu.VMEM((key_n, key_m, part, cut), BF16),
        pltpu.VMEM((key_n, key_m, part, cut), BF16),
        pltpu.VMEM((key_m, part, cut), F32),
        pltpu.VMEM((key_m, part, cut), BF16),
        pltpu.VMEM((key_m, part, cut), BF16),
        pltpu.VMEM((key_m, key_n, part, rest), BF16),
        pltpu.VMEM((key_m, key_n, part, rest), BF16),
        pltpu.VMEM((key_n, part, rest), F32),
        pltpu.VMEM((key_n, part, rest), BF16),
        pltpu.VMEM((key_n, part, rest), BF16),
        dma,
    ]
    for shape in (
        (tgt_n, chunks), (tgt_n, chunks), (tgt_n, chunks), (tgt_n,), (tgt_n,),
        (src_n,), (src_n,), (src_n,), (tgt_n,), (tgt_n,), (src_n, 2), (src_n, 2),
        (tp_n, 2), (tp_n, 2), (key_n,), (key_n,), (key_m,), (key_m,),
        (key_m,), (key_m,), (key_n,), (key_n,),
    ):
        scratch.append(dma(shape))
    query_grad, kv_half, key_grad = pl.pallas_call(
        functools.partial(kernel, tgt_n, src_n, key_n, tp_n, src_rows * sp_n),
        out_shape=(
            jax.ShapeDtypeStruct((rows, width), F32),
            jax.ShapeDtypeStruct((src_rows, 2 * kv_width), BF16),
            jax.ShapeDtypeStruct((part, columns), F32),
        ),
        in_specs=[vmem] * 6 + [pl.BlockSpec(memory_space=pl.ANY)],
        out_specs=(vmem, vmem, vmem),
        scratch_shapes=scratch,
        compiler_params=pltpu.CompilerParams(
            collective_id=0, has_side_effects=True, vmem_limit_bytes=60 * 2**20
        ),
        name="attention_grads",
    )(queries, attn_out, out_grad, row_lse.T, saved_keys, saved_values, source)
    source_grad = dot_nt(kv_half[:, :kv_width], key_weight) + dot_nt(
        kv_half[:, kv_width:], value_weight
    )
    return (query_grad, source_grad, key_grad)


def solution(mesh):
    sp_n, tp_n = mesh.shape["sp"], mesh.shape["tp"]
    src_n = 2 ** (int(math.log2(sp_n)) // 2)
    in_specs = (
        P("sp", "tp"),
        P("sp", "tp"),
        P("sp", "tp"),
        P("sp", "tp"),
        P("sp", "tp"),
        P("sp", None),
        P("sp", None),
        P("tp", None),
        P("tp", None),
    )
    out_specs = (P("sp", "tp"), P("sp", "tp"), P("sp", "tp"))
    return jax.shard_map(
        functools.partial(shards, sp_n // src_n, src_n, tp_n),
        mesh=mesh, in_specs=in_specs, out_specs=out_specs, check_vma=False,
    )
```

time: 79.8 us -> 72 us (0.902)
  Pallas kernels: 73 us -> 65.2 us
    pallas_call x1, Pallas kernels: 73 us -> 65.2 us  [shards(): pl.pallas_call(functools.partial(kernel, tgt_n, src_n, key_n, tp_n, src_r...]
where the time goes in v2:
time: 72 us; the launch traced here: 71.8 us
  Pallas kernels  65.2 us (91%)
  matrix products  4.52 us (6%)
  local copies, waits for them, and re-layouts  1.38 us (2%)
    pallas_call x1, Pallas kernels, shards(): pl.pallas_call(functools.partial(kernel, tgt_n, src_n, key_n, tp_n, src_r...  65.2 us
    dot_general x2, matrix products, dot_nt(): lax.dot_general(left, right, (((1,), (1,)), ((), ())), preferred_element_...  4.52 us

profile of v2, /device:TPU:0, one launch (start us, length us, event | category | flops | bytes accessed | tf_op | source)
XLA Modules:
  0.0 71.8 jit_solution(16970199960473547473)
XLA Ops:
  0.6 0.0 copy-start
  0.6 0.0 copy-start.1
  0.7 65.2 %attention_grads.1 = (f32[128,512]{1,0:T(8,128)}, bf16[512,512]{1,0:T(8,128)(2,1)}, f32[16,2048]{1,0:T(8,128)}) custom-call(bf16[128,512]{1,0:T(8,128)(2,1)} %q_ref.1, bf16[128,512]{1,0:T(8,128)(2,1)} %o_ref.1, bf16[128,512]{1,0:T(8,128)(2,1)} %d_ref.1, f32[4,128]{1,0:T(4,128)} %bitcast.3, bf16[512,256]{1,0:T(8,128)(2,1)} %key_ref.1, ...), custom_call_target="tpu_custom_call" | custom-call | tf_op jit(solution)/shard_map/attention_grads/pallas_call | solution.py:392
  65.8 0.0 copy-start.2
  65.8 0.0 copy-done
  65.9 1.7 %fusion.1 = f32[512,2048]{1,0:T(8,128)S(1)} fusion(bf16[2048,256]{1,0:T(8,128)(2,1)S(1)} %copy-done, bf16[512,512]{1,0:T(8,128)(2,1)} %get-tuple-element.7), kind=kOutput, calls=%fused_computation.2 | convolution fusion | flops 536870912 | bytes 5505024 | tf_op jit(solution)/shard_map/dot_general | solution.py:21
  67.6 0.0 copy-done.1
  67.6 0.0 copy-done.2
  67.6 0.0 copy-start.3
  67.6 0.0 copy-start.4
  67.7 2.8 %convolution_add_fusion = f32[512,2048]{1,0:T(8,128)} fusion(f32[512,2048]{1,0:T(8,128)S(1)} %fusion.1, bf16[2048,256]{1,0:T(8,128)(2,1)S(1)} %copy-done.1, bf16[512,512]{1,0:T(8,128)(2,1)S(1)} %copy-done.2), kind=kOutput, calls=%fused_computation | convolution fusion | flops 537919488 | bytes 9699328 | tf_op jit(solution)/shard_map/dot_general | solution.py:21
  70.4 0.0 copy-done.3
  70.4 0.7 copy.14
  71.1 0.0 copy-done.4
  71.1 0.7 copy.15
Async XLA Ops:
  0.6 65.2 %copy-start = (bf16[2048,256]{1,0:T(8,128)(2,1)S(1)}, bf16[2048,256]{1,0:T(8,128)(2,1)}, u32[]{:S(2)}) copy-start(bf16[2048,256]{1,0:T(8,128)(2,1)} %param.16) | copy-start | bytes 3145732
  0.6 67.0 %copy-start.1 = (bf16[2048,256]{1,0:T(8,128)(2,1)S(1)}, bf16[2048,256]{1,0:T(8,128)(2,1)}, u32[]{:S(2)}) copy-start(bf16[2048,256]{1,0:T(8,128)(2,1)} %param.17) | copy-start | bytes 3145732
  65.8 1.8 %copy-start.2 = (bf16[512,512]{1,0:T(8,128)(2,1)S(1)}, bf16[512,512]{1,0:T(8,128)(2,1)}, u32[]{:S(2)}) copy-start(bf16[512,512]{1,0:T(8,128)(2,1)} %get-tuple-element.7) | copy-start | bytes 1572868
  67.6 2.8 %copy-start.3 = (f32[128,512]{1,0:T(8,128)S(1)}, f32[128,512]{1,0:T(8,128)}, u32[]{:S(2)}) copy-start(f32[128,512]{1,0:T(8,128)} %get-tuple-element.12) | copy-start | bytes 786436
  67.6 3.5 %copy-start.4 = (f32[16,2048]{1,0:T(8,128)S(1)}, f32[16,2048]{1,0:T(8,128)}, u32[]{:S(2)}) copy-start(f32[16,2048]{1,0:T(8,128)} %get-tuple-element.14) | copy-start | bytes 393220

commit v3 on v2

--- a/solution.py
+++ b/solution.py
@@ -35,9 +35,9 @@
     tgt_n, src_n, key_n, tp_n, src_total,
     q_ref, o_ref, d_ref, lse_ref, key_ref, value_ref, source_ref,
     dq_ref, kv_ref, kg_ref,
-    qd, stats, kvs, dk, dv, dq_acc, dq_out, dq_in, g_out, g_in, tp_own, tp_in,
+    qd, stats, kvs, dk, dv, dq_acc, dq_out, dq_in, dq_via, g_out, g_in, tp_own, tp_in,
     src, a_out, a_in, a2_own, a2_out, a2_in, b_out, b_in, b2_own, b2_out, b2_in,
-    copy_sem, qd_s, qd_r, rq_s, st_s, st_r, kv_s, kv_r, rkv_s, dq_s, dq_r, g_s, g_r, tp_s, tp_r,
+    copy_sem, qd_s, qd_r, rq_s, st_s, st_r, kv_s, kv_r, rkv_s, dq_s, dq_r, via_r, g_s, g_r, tp_s, tp_r,
     a_s, a_r, a2_s, a2_r, b_s, b_r, b2_s, b2_r,
 ):
     sp = lax.axis_index("sp")
@@ -63,7 +63,7 @@
     tp_peers = [lax.rem(tp + k, tp_n) for k in range(1, tp_n)]
     rows = q_ref.shape[0]
     heads = q_ref.shape[1] // HEAD_DIM
-    chunks = qd.shape[1]
+    chunks = stats.shape[1]
     per_chunk = heads // chunks
     src_rows = key_ref.shape[0]
     per_key = HEADS // KV_HEADS
@@ -100,27 +100,6 @@
         )
     for p in tp_peers:
         pl.semaphore_signal(barrier, inc=1, device_id=tp_dev(p), device_id_type=MESH)
-    pl.semaphore_wait(barrier, sp_n + tp_n - 2)
-
-    def send_q(t):
-        for c in range(chunks):
-            for h in range(per_chunk):
-                for i, ref in enumerate((q_ref, d_ref)):
-                    remote(
-                        ref.at[:, pl.ds((c * per_chunk + h) * HEAD_DIM, HEAD_DIM)],
-                        qd.at[me_t, c, i, pl.ds(h * rows, rows), :],
-                        qd_s.at[t, c], qd_r.at[me_t, c], t_dev(t),
-                    ).start()
-
-    for s in far_s + [near_s]:
-        for i, ref in enumerate((key_ref, value_ref)):
-            remote(
-                ref.at[:, pl.ds(kv_col, HEAD_DIM)], kvs.at[me_s, i],
-                kv_s.at[s], kv_r.at[me_s], s_dev(s),
-            ).start()
-    for t in far_t + [near_t]:
-        send_q(t)
-
     ones = jnp.ones((8, HEAD_DIM), F32)
     for h in range(heads):
         cols = pl.ds(h * HEAD_DIM, HEAD_DIM)
@@ -129,19 +108,40 @@
         delta = dot_nt(ones, prod, lax.Precision.HIGHEST)
         stats[me_t, c, 0:1, span] = lse_ref[h : h + 1, :] * LOG2E
         stats[me_t, c, 1:2, span] = delta[0:1, :]
-        qd[me_t, c, 0, span, :] = q_ref[:, cols]
-        qd[me_t, c, 1, span, :] = d_ref[:, cols]
     kvs[me_s, 0] = key_ref[:, pl.ds(kv_col, HEAD_DIM)]
     kvs[me_s, 1] = value_ref[:, pl.ds(kv_col, HEAD_DIM)]
+    qd[me_t, 0] = q_ref[...]
+    qd[me_t, 1] = d_ref[...]
     dk[...] = jnp.zeros_like(dk)
     dv[...] = jnp.zeros_like(dv)
     dq_acc[...] = jnp.zeros_like(dq_acc)
+    pl.semaphore_wait(barrier, sp_n + tp_n - 2)
+
+    def send_q(t):
+        for i, ref in enumerate((q_ref, d_ref)):
+            remote(ref, qd.at[me_t, i], qd_s.at[t, i], qd_r.at[me_t, i], t_dev(t)).start()
+
+    for s in far_s + [near_s]:
+        remote(kvs.at[me_s], kvs.at[me_s], kv_s.at[s], kv_r.at[me_s], s_dev(s)).start()
+    for t in far_t + [near_t]:
+        send_q(t)
+
     for t in t_peers:
         remote(stats.at[me_t], stats.at[me_t], st_s.at[t], st_r.at[me_t], t_dev(t)).start()
 
+    def stack(t, i, c):
+        low = c * per_chunk
+        return jnp.concatenate(
+            [
+                qd[t, i, :, pl.ds(pl.multiple_of((low + h) * HEAD_DIM, HEAD_DIM), HEAD_DIM)]
+                for h in range(per_chunk)
+            ],
+            axis=0,
+        )
+
     def tile(t, s):
         def body(c, carry):
-            q, d = qd[t, c, 0], qd[t, c, 1]
+            q, d = stack(t, 0, c), stack(t, 1, c)
             k, v = kvs[s, 0], kvs[s, 1]
             scores = dot_nt(k, q)
             probs = jnp.exp2(scores * (scale * LOG2E) - stats[t, c, 0:1, :])
@@ -171,9 +171,8 @@
     def relay_kv(s):
         return remote(kvs.at[s], kvs.at[s], rkv_s.at[s], kv_r.at[s], s_dev(near_s))
 
-    def send_dq(t):
-        dq_out[t] = (dq_acc[t] * scale).astype(BF16)
-        remote(dq_out.at[t], dq_in.at[me_t], dq_s.at[t], dq_r.at[me_t], t_dev(t)).start()
+    def dq_copy(t):
+        return remote(dq_out.at[t], dq_in.at[me_t], dq_s.at[t], dq_r.at[me_t], t_dev(t))
 
     def send_g(s, i):
         g_out[s, i] = dv[s].astype(BF16) if i else (dk[s] * scale).astype(BF16)
@@ -187,14 +186,14 @@
         relay_kv(s).start()
     got_kv(near_s)
     tile(me_t, near_s)
-    for c in range(chunks):
+    for c in range(2):
         for t in far_t:
             got_q(t, c)
             relay_q(t, c).start()
         if c == 0:
             for s in far_s:
                 tile(me_t, s)
-            for c2 in range(chunks):
+            for c2 in range(2):
                 got_q(near_t, c2)
             got_stats(near_t)
     for s in [me_s, near_s] + far_s:
@@ -207,10 +206,10 @@
         got_kv(s)
         for t in [near_t] + far_t + [me_t]:
             tile(t, s)
-    for t in [near_t] + far_t:
-        send_dq(t)
+    dq_out[near_t] = (dq_acc[near_t] * scale).astype(BF16)
+    dq_copy(near_t).start()
     for n, t in enumerate(diag_t):
-        for c in range(chunks):
+        for c in range(2):
             got_q(t, c)
         got_stats(t)
         for s in far_s + diag_s + [near_s]:
@@ -221,7 +220,12 @@
             for s in far_s + diag_s + [near_s]:
                 send_g(s, 1)
         tile(t, me_s)
-        send_dq(t)
+        dq_out[t] = (dq_acc[t] * scale).astype(BF16)
+        remote(dq_out.at[t], dq_via.at[t], dq_s.at[t], via_r.at[t], t_dev(near_t)).start()
+    for t in far_t:
+        remote(dq_out.at[t], dq_via.at[t], dq_s.at[t], via_r.at[t], t_dev(near_t)).wait_recv()
+        dq_out[t] = (dq_acc[t] * scale + dq_via[t].astype(F32)).astype(BF16)
+        dq_copy(t).start()
 
     def reduce_g(i):
         total = dv[me_s] if i else dk[me_s] * scale
@@ -274,7 +278,7 @@
     reduce_g(1)
     gather_g(1)
     dq_total = dq_acc[me_t] * scale
-    for t in t_peers:
+    for t in [near_t] + far_t:
         remote(dq_in.at[t], dq_in.at[t], dq_s.at[t], dq_r.at[t], t_dev(t)).wait_recv()
         dq_total += dq_in[t].astype(F32)
     for h in range(heads):
@@ -309,10 +313,10 @@
     kg_ref[:, :cut] = total
 
     for t in far_t + [near_t]:
-        for c in range(chunks):
+        for c in range(2):
             remote(qd.at[t, c], qd.at[t, c], qd_s.at[t, c], qd_r.at[t, c], t_dev(t)).wait_send()
     for t in far_t:
-        for c in range(chunks):
+        for c in range(2):
             relay_q(t, c).wait_send()
     for t in t_peers:
         remote(stats.at[t], stats.at[t], st_s.at[t], st_r.at[t], t_dev(t)).wait_send()
@@ -357,12 +361,13 @@
     dma = pltpu.SemaphoreType.DMA
     vmem = pl.BlockSpec(memory_space=pltpu.VMEM)
     scratch = [
-        pltpu.VMEM((tgt_n, chunks, 2, stacked, HEAD_DIM), BF16),
+        pltpu.VMEM((tgt_n, 2, rows, width), BF16),
         pltpu.VMEM((tgt_n, chunks, 8, stacked), F32),
         pltpu.VMEM((src_n, 2, src_rows, HEAD_DIM), BF16),
         pltpu.VMEM((src_n, src_rows, HEAD_DIM), F32),
         pltpu.VMEM((src_n, src_rows, HEAD_DIM), F32),
         pltpu.VMEM((tgt_n, chunks, stacked, HEAD_DIM), F32),
+        pltpu.VMEM((tgt_n, chunks, stacked, HEAD_DIM), BF16),
         pltpu.VMEM((tgt_n, chunks, stacked, HEAD_DIM), BF16),
         pltpu.VMEM((tgt_n, chunks, stacked, HEAD_DIM), BF16),
         pltpu.VMEM((src_n, 2, src_rows, HEAD_DIM), BF16),
@@ -383,8 +388,8 @@
         dma,
     ]
     for shape in (
-        (tgt_n, chunks), (tgt_n, chunks), (tgt_n, chunks), (tgt_n,), (tgt_n,),
-        (src_n,), (src_n,), (src_n,), (tgt_n,), (tgt_n,), (src_n, 2), (src_n, 2),
+        (tgt_n, 2), (tgt_n, 2), (tgt_n, 2), (tgt_n,), (tgt_n,),
+        (src_n,), (src_n,), (src_n,), (tgt_n,), (tgt_n,), (tgt_n,), (src_n, 2), (src_n, 2),
         (tp_n, 2), (tp_n, 2), (key_n,), (key_n,), (key_m,), (key_m,),
         (key_m,), (key_m,), (key_n,), (key_n,),
     ):

time: 72 us -> 69.4 us (0.964)
  Pallas kernels: 65.2 us -> 62.7 us
    pallas_call x1, Pallas kernels: 65.2 us -> 62.7 us  [shards(): pl.pallas_call(functools.partial(kernel, tgt_n, src_n, key_n, tp_n, src_r...]
where the time goes in v3:
time: 69.4 us; the launch traced here: 69.3 us
  Pallas kernels  62.7 us (90%)
  matrix products  4.52 us (7%)
  local copies, waits for them, and re-layouts  1.38 us (2%)
  between operations  0.71 us (1%)
    pallas_call x1, Pallas kernels, shards(): pl.pallas_call(functools.partial(kernel, tgt_n, src_n, key_n, tp_n, src_r...  62.7 us
    dot_general x2, matrix products, dot_nt(): lax.dot_general(left, right, (((1,), (1,)), ((), ())), preferred_element_...  4.52 us

profile of v3, /device:TPU:0, one launch (start us, length us, event | category | flops | bytes accessed | tf_op | source)
XLA Modules:
  0.0 69.3 jit_solution(11537138999329517832)
XLA Ops:
  0.6 0.0 copy-start
  0.6 0.0 copy-start.1
  0.7 62.7 %attention_grads.1 = (f32[128,512]{1,0:T(8,128)}, bf16[512,512]{1,0:T(8,128)(2,1)}, f32[16,2048]{1,0:T(8,128)}) custom-call(bf16[128,512]{1,0:T(8,128)(2,1)} %q_ref.1, bf16[128,512]{1,0:T(8,128)(2,1)} %o_ref.1, bf16[128,512]{1,0:T(8,128)(2,1)} %d_ref.1, f32[4,128]{1,0:T(4,128)} %bitcast.3, bf16[512,256]{1,0:T(8,128)(2,1)} %key_ref.1, ...), custom_call_target="tpu_custom_call" | custom-call | tf_op jit(solution)/shard_map/attention_grads/pallas_call | solution.py:397
  63.3 0.0 copy-start.2
  63.3 0.0 copy-done
  63.4 1.7 %fusion.1 = f32[512,2048]{1,0:T(8,128)S(1)} fusion(bf16[2048,256]{1,0:T(8,128)(2,1)S(1)} %copy-done, bf16[512,512]{1,0:T(8,128)(2,1)} %get-tuple-element.7), kind=kOutput, calls=%fused_computation.2 | convolution fusion | flops 536870912 | bytes 5505024 | tf_op jit(solution)/shard_map/dot_general | solution.py:21
  65.1 0.0 copy-done.1
  65.1 0.0 copy-done.2
  65.1 0.0 copy-start.3
  65.1 0.0 copy-start.4
  65.1 2.8 %convolution_add_fusion = f32[512,2048]{1,0:T(8,128)} fusion(f32[512,2048]{1,0:T(8,128)S(1)} %fusion.1, bf16[2048,256]{1,0:T(8,128)(2,1)S(1)} %copy-done.1, bf16[512,512]{1,0:T(8,128)(2,1)S(1)} %copy-done.2), kind=kOutput, calls=%fused_computation | convolution fusion | flops 537919488 | bytes 9699328 | tf_op jit(solution)/shard_map/dot_general | solution.py:21
  67.9 0.0 copy-done.3
  67.9 0.7 %copy.14 = f32[128,512]{1,0:T(8,128)} copy(f32[128,512]{1,0:T(8,128)S(1)} %copy-done.3) | data formatting | bytes 524288
  68.6 0.0 copy-done.4
  68.6 0.7 copy.15
Async XLA Ops:
  0.6 62.7 %copy-start = (bf16[2048,256]{1,0:T(8,128)(2,1)S(1)}, bf16[2048,256]{1,0:T(8,128)(2,1)}, u32[]{:S(2)}) copy-start(bf16[2048,256]{1,0:T(8,128)(2,1)} %param.16) | copy-start | bytes 3145732
  0.6 64.5 %copy-start.1 = (bf16[2048,256]{1,0:T(8,128)(2,1)S(1)}, bf16[2048,256]{1,0:T(8,128)(2,1)}, u32[]{:S(2)}) copy-start(bf16[2048,256]{1,0:T(8,128)(2,1)} %param.17) | copy-start | bytes 3145732
  63.3 1.8 %copy-start.2 = (bf16[512,512]{1,0:T(8,128)(2,1)S(1)}, bf16[512,512]{1,0:T(8,128)(2,1)}, u32[]{:S(2)}) copy-start(bf16[512,512]{1,0:T(8,128)(2,1)} %get-tuple-element.7) | copy-start | bytes 1572868
  65.1 2.8 %copy-start.3 = (f32[128,512]{1,0:T(8,128)S(1)}, f32[128,512]{1,0:T(8,128)}, u32[]{:S(2)}) copy-start(f32[128,512]{1,0:T(8,128)} %get-tuple-element.12) | copy-start | bytes 786436
  65.1 3.5 %copy-start.4 = (f32[16,2048]{1,0:T(8,128)S(1)}, f32[16,2048]{1,0:T(8,128)}, u32[]{:S(2)}) copy-start(f32[16,2048]{1,0:T(8,128)} %get-tuple-element.14) | copy-start | bytes 393220

commit v4 on v3

--- a/solution.py
+++ b/solution.py
@@ -341,6 +341,53 @@
             remote(
                 tp_own.at[i], tp_in.at[p, i], tp_s.at[p, i], tp_r.at[p, i], tp_dev(p)
             ).wait_send()
+
+
+def finish_kernel(
+    kv_hbm, kw_hbm, vw_hbm, dq_hbm, kg_hbm, out_ref, dq_out, kg_out,
+    kv, kw, vw, dq, kg, buf, in_sems, w_sems, out_sems, pass_sems,
+):
+    half = kw.shape[1]
+    width = buf.shape[2]
+    count = buf.shape[0]
+    load = pltpu.make_async_copy(kv_hbm, kv, in_sems.at[0])
+    load.start()
+    loads = []
+    for n in range(count):
+        cols = pl.ds(n * width, width)
+        loads.append(
+            [
+                pltpu.make_async_copy(ref.at[cols], to.at[cols], w_sems.at[n, i])
+                for i, (ref, to) in enumerate(((kw_hbm, kw), (vw_hbm, vw)))
+            ]
+        )
+        for copy in loads[n]:
+            copy.start()
+    dq_in = pltpu.make_async_copy(dq_hbm, dq, in_sems.at[1])
+    kg_in = pltpu.make_async_copy(kg_hbm, kg, in_sems.at[2])
+    dq_in.start()
+    kg_in.start()
+    load.wait()
+    copies = []
+    for n in range(count):
+        cols = slice(n * width, (n + 1) * width)
+        for copy in loads[n]:
+            copy.wait()
+        buf[n] = dot_nt(kv[:, :half], kw[cols]) + dot_nt(kv[:, half:], vw[cols])
+        copies.append(
+            pltpu.make_async_copy(
+                buf.at[n], out_ref.at[:, pl.ds(n * width, width)], out_sems.at[n]
+            )
+        )
+        copies[n].start()
+    dq_in.wait()
+    copies.append(pltpu.make_async_copy(dq, dq_out, pass_sems.at[0]))
+    copies[-1].start()
+    kg_in.wait()
+    copies.append(pltpu.make_async_copy(kg, kg_out, pass_sems.at[1]))
+    copies[-1].start()
+    for copy in copies:
+        copy.wait()
 
 
 def shards(
@@ -409,9 +456,33 @@
         ),
         name="attention_grads",
     )(queries, attn_out, out_grad, row_lse.T, saved_keys, saved_values, source)
-    source_grad = dot_nt(kv_half[:, :kv_width], key_weight) + dot_nt(
-        kv_half[:, kv_width:], value_weight
-    )
+    local_columns = key_weight.shape[0]
+    blocks = local_columns // math.gcd(local_columns, 256)
+    hbm = pl.BlockSpec(memory_space=pl.ANY)
+    source_grad, query_grad, key_grad = pl.pallas_call(
+        finish_kernel,
+        out_shape=(
+            jax.ShapeDtypeStruct((src_rows, local_columns), F32),
+            jax.ShapeDtypeStruct((rows, width), F32),
+            jax.ShapeDtypeStruct((part, columns), F32),
+        ),
+        in_specs=[hbm] * 5,
+        out_specs=(hbm, hbm, hbm),
+        scratch_shapes=[
+            pltpu.VMEM((src_rows, 2 * kv_width), BF16),
+            pltpu.VMEM((local_columns, kv_width), BF16),
+            pltpu.VMEM((local_columns, kv_width), BF16),
+            pltpu.VMEM((rows, width), F32),
+            pltpu.VMEM((part, columns), F32),
+            pltpu.VMEM((blocks, src_rows, local_columns // blocks), F32),
+            dma((3,)),
+            dma((blocks, 2)),
+            dma((blocks,)),
+            dma((2,)),
+        ],
+        compiler_params=pltpu.CompilerParams(vmem_limit_bytes=60 * 2**20),
+        name="source_grads",
+    )(kv_half, key_weight, value_weight, query_grad, key_grad)
     return (query_grad, source_grad, key_grad)
 
 

time: 69.4 us -> 69.8 us (level)
  Pallas kernels: 62.7 us -> 69 us
  matrix products: 4.52 us -> 0 us
  local copies, waits for them, and re-layouts: 1.38 us -> 0 us
    pallas_call x0 -> x1, Pallas kernels: none -> 6.46 us  [shards(): pl.pallas_call(finish_kernel, out_shape=(jax.ShapeDtypeStruct((src_rows,...]
    dot_general x2 -> x0, matrix products: 4.52 us -> none  [dot_nt(): lax.dot_general(left, right, (((1,), (1,)), ((), ())), preferred_element_...]
    unnamed x12 -> x0, local copies, waits for them, and re-layouts: 1.38 us -> none
where the time goes in v4:
time: 69.8 us; the launch traced here: 69.6 us
  Pallas kernels  69 us (99%)
    pallas_call x1, Pallas kernels, shards(): pl.pallas_call(functools.partial(kernel, tgt_n, src_n, key_n, tp_n, src_r...  62.5 us
    pallas_call x1, Pallas kernels, shards(): pl.pallas_call(finish_kernel, out_shape=(jax.ShapeDtypeStruct((src_rows,...  6.46 us

profile of v4, /device:TPU:0, one launch (start us, length us, event | category | flops | bytes accessed | tf_op | source)
XLA Modules:
  0.0 69.6 jit_solution(2061482263440978141)
XLA Ops:
  0.6 62.5 %attention_grads.1 = (f32[128,512]{1,0:T(8,128)}, bf16[512,512]{1,0:T(8,128)(2,1)}, f32[16,2048]{1,0:T(8,128)}) custom-call(bf16[128,512]{1,0:T(8,128)(2,1)} %q_ref.1, bf16[128,512]{1,0:T(8,128)(2,1)} %o_ref.1, bf16[128,512]{1,0:T(8,128)(2,1)} %d_ref.1, f32[4,128]{1,0:T(4,128)} %bitcast.1, bf16[512,256]{1,0:T(8,128)(2,1)} %key_ref.1, ...), custom_call_target="tpu_custom_call" | custom-call | tf_op jit(solution)/shard_map/attention_grads/pallas_call | solution.py:444
  63.2 6.5 %source_grads.1 = (f32[512,2048]{1,0:T(8,128)}, f32[128,512]{1,0:T(8,128)}, f32[16,2048]{1,0:T(8,128)}) custom-call(bf16[512,512]{1,0:T(8,128)(2,1)} %get-tuple-element.9.kv_hbm, bf16[2048,256]{1,0:T(8,128)(2,1)} %kw_hbm.1, bf16[2048,256]{1,0:T(8,128)(2,1)} %vw_hbm.1, f32[128,512]{1,0:T(8,128)} %get-tuple-element.10.dq_hbm, f32[16,2048]{1,0:T(8,128)} %get-tuple-element.11.kg_hbm), custom_call_target="tpu_custom_call" | custom-call | tf_op jit(solution)/shard_map/source_grads/pallas_call | solution.py:462
